TPU v7x, 32 devices: a whole 2x2x4 slice. The times are simulated.
32 devices in a mesh: sp: 16 (over z, y, x), tp: 2 (over core).
Axes of the slice: x: 2, y: 2, z: 4, core: 2. Of those that a mesh axis runs over, the one named last changes fastest.
Arguments:
- query_rows: bfloat16 [4096, 1024], P('sp', 'tp'), may hold values from -26 to 26
- key_rows: bfloat16 [4096, 128], P('sp', 'tp'), may hold values from -26 to 26
- value_head_rows: bfloat16 [4096, 128], P('sp', 'tp'), may hold values from -6 to 6
- sink_logit_head: float32 [16], P('tp'), may hold values from -6 to 6
- out_weight: bfloat16 [1024, 2048], P('tp'), may hold values from -0.1875 to 0.1875
- residual: bfloat16 [4096, 2048], P(('sp', 'tp')), may hold values from -6 to 6
- norm_gain: float32 [2048], replicated, may hold values from 0.1 to 1.9
- routes: int32 [4096, 2], P(('sp', 'tp')), may hold values from 0 to 15, all different within a row; in each aligned block of 128 rows (0 to 127, 128 to 255, ...) at most 24 rows name the same one
- route_weights: float32 [4096, 2], P(('sp', 'tp')), may hold values from 0.1 to 1
- gate_proj: bfloat16 [16, 2048, 3584], P('sp', None, 'tp'), may hold values from -0.125 to 0.125
- up_proj: bfloat16 [16, 2048, 3584], P('sp', None, 'tp'), may hold values from -0.125 to 0.125
- down_proj: bfloat16 [16, 3584, 2048], P('sp', 'tp'), may hold values from -0.09375 to 0.09375
Outputs:
- output: bfloat16 [4096, 2048], P(('sp', 'tp'))
Inputs may be any that keep to these rules, and one draw needn't show every extreme that they name: `routes`: A row names 2 different experts. Among the rows of one device no expert is named more than 24 times, a bound that some block reaches on some devices.
All inputs are finite; a program needn't handle non-finite values.
Results may differ from a plain program's by a relative error of at most 0.0055.
Values may be sent and summed in bfloat16 or wider, within the bound.
No kernel may reach another device: no remote copies, remote signals or barrier semaphores. Data moves between devices by JAX's collectives and lax.ppermute only.
A program may use at most 128 MiB of HBM per device.

v0:
```python
import jax
import jax.numpy as jnp
from jax import lax
from jax.sharding import PartitionSpec as P

QUERY_HEADS = 16
KEY_VALUE_HEADS = 2
HEAD_SIZE = 64
TOP = 2
WINDOW_KEYS = 128


def from_behind(block, axis, distance):
    devices = range(lax.axis_size(axis))
    route = [(i - distance, i) for i in devices if i - distance in devices]
    return lax.ppermute(block, axis, route)


def on_device(
    query_rows,
    key_rows,
    value_head_rows,
    sink_logit_head,
    out_weight,
    residual,
    norm_gain,
    routes,
    route_weights,
    gate_proj,
    up_proj,
    down_proj,
):
    length = query_rows.shape[0]
    query_group = QUERY_HEADS // KEY_VALUE_HEADS
    width = key_rows.shape[1]
    local_kv = width // HEAD_SIZE
    local_heads = local_kv * query_group
    sp_index = lax.axis_index("sp")
    tp_index = lax.axis_index("tp")
    tail = jnp.concatenate(
        [key_rows[length - WINDOW_KEYS :], value_head_rows[length - WINDOW_KEYS :]], axis=1
    )
    before = from_behind(tail, "sp", 1)
    key_all = jnp.concatenate([before[:, :width], key_rows], axis=0)
    value_all = jnp.concatenate([before[:, width:], value_head_rows], axis=0)
    score_matrix = jnp.einsum(
        "rjwh,cjh->jwrc",
        query_rows.reshape(length, local_kv, query_group, HEAD_SIZE),
        key_all.reshape(-1, local_kv, HEAD_SIZE),
        preferred_element_type=jnp.float32,
    ) * HEAD_SIZE ** (-0.5)
    query_pos = sp_index * length + jnp.arange(length, dtype=jnp.int32)
    key_pos = sp_index * length - WINDOW_KEYS + jnp.arange(length + WINDOW_KEYS, dtype=jnp.int32)
    distance = query_pos[:, None] - key_pos[None, :]
    inside = (distance >= 0) & (distance < WINDOW_KEYS) & (key_pos[None, :] >= 0)
    head_ids = (tp_index * local_heads + jnp.arange(local_heads, dtype=jnp.int32)).astype(
        jnp.float32
    )
    slope_values = jnp.exp2(-8.0 * (head_ids + 1.0) / QUERY_HEADS).reshape(local_kv, query_group)
    score_matrix = (
        score_matrix - slope_values[:, :, None, None] * distance.astype(jnp.float32)[None, None]
    )
    score_matrix = jnp.where(inside[None, None], score_matrix, -jnp.inf)
    sink_portion = sink_logit_head.reshape(local_kv, query_group)[:, :, None]
    peak = jnp.maximum(jnp.max(score_matrix, axis=-1), sink_portion)
    expd = jnp.exp(score_matrix - peak[..., None])
    denom = jnp.sum(expd, axis=-1) + jnp.exp(sink_portion - peak)
    probabilities = (expd / denom[..., None]).astype(jnp.bfloat16)
    attended = (
        jnp.einsum(
            "wfbt,twj->bwfj",
            probabilities,
            value_all.reshape(-1, local_kv, HEAD_SIZE),
            preferred_element_type=jnp.float32,
        )
        .reshape(length, local_heads * HEAD_SIZE)
        .astype(jnp.bfloat16)
    )
    own_rows = length // lax.axis_size("tp")
    projected = lax.psum_scatter(
        jnp.dot(attended, out_weight, preferred_element_type=jnp.float32),
        "tp",
        scatter_dimension=0,
        tiled=True,
    )
    mixed = residual.astype(jnp.float32) + projected
    scale = lax.rsqrt(jnp.mean(mixed * mixed, axis=-1, keepdims=True) + 1e-05)
    normed = (mixed * scale * norm_gain).astype(jnp.bfloat16)
    n_sp = lax.axis_size("sp")
    n_tp = lax.axis_size("tp")
    capacity = 3 * own_rows * TOP // (2 * n_sp)
    chosen = routes.reshape(-1)
    onehot = (chosen[:, None] == jnp.arange(n_sp, dtype=jnp.int32)[None, :]).astype(jnp.int32)
    running = jnp.cumsum(onehot, axis=0)
    rank_in = jnp.sum(onehot * running, axis=1) - 1
    slot_index = chosen * capacity + rank_in
    slot_ids = jnp.arange(n_sp * capacity, dtype=jnp.int32)
    select = jnp.any(
        slot_index.reshape(own_rows, TOP)[None, :, :] == slot_ids[:, None, None], axis=-1
    )
    dispatch = jnp.dot(
        select.astype(jnp.bfloat16), normed, preferred_element_type=jnp.float32
    ).astype(jnp.bfloat16)
    model_width = dispatch.shape[1]
    landed = lax.all_to_all(
        dispatch.reshape(n_sp, capacity, model_width), "sp", split_axis=0, concat_axis=0, tiled=True
    )
    arrived = lax.all_gather(
        landed.reshape(n_sp, 1, capacity, model_width), "tp", axis=1, tiled=True
    )
    rows_in = arrived.reshape(-1, model_width)
    gate = jnp.dot(rows_in, gate_proj[0], preferred_element_type=jnp.float32)
    upper = jnp.dot(rows_in, up_proj[0], preferred_element_type=jnp.float32)
    hidden = (jax.nn.silu(gate) * upper).astype(jnp.bfloat16)
    partial_out = jnp.dot(hidden, down_proj[0], preferred_element_type=jnp.float32)
    partial_out = partial_out.reshape(n_sp, n_tp, capacity, model_width)
    summed = lax.psum_scatter(
        partial_out.astype(jnp.bfloat16), "tp", scatter_dimension=1, tiled=True
    )
    expert_out = summed.reshape(n_sp, capacity, model_width)
    returned = lax.all_to_all(expert_out, "sp", split_axis=0, concat_axis=0, tiled=True)
    picked = returned.reshape(n_sp * capacity, model_width)[slot_index].reshape(
        own_rows, TOP, model_width
    )
    moe_sum = jnp.sum(route_weights[:, :, None] * picked.astype(jnp.float32), axis=1)
    return (mixed + moe_sum).astype(jnp.bfloat16)


def solution(mesh):
    placed = (
        P("sp", "tp"),
        P("sp", "tp"),
        P("sp", "tp"),
        P("tp"),
        P("tp", None),
        P(("sp", "tp"), None),
        P(),
        P(("sp", "tp"), None),
        P(("sp", "tp"), None),
        P("sp", None, "tp"),
        P("sp", None, "tp"),
        P("sp", "tp", None),
    )
    return jax.shard_map(
        on_device, mesh=mesh, in_specs=placed, out_specs=P(("sp", "tp"), None), check_vma=False
    )
```

profile of v0, /device:TPU:12, one launch (start us, length us, event | category | flops | bytes accessed | tf_op | source)
XLA Modules:
  0.0 209.4 jit_solution(3881032120100905958)
XLA Ops:
  6.5 0.0 copy-start
  6.5 0.0 reduce-scatter.3.cloned.1.call-start
  6.5 0.9 slice.18
  7.4 0.7 slice.19
  8.1 3.4 %collective-permute-start = (bf16[128,128]{0,1:T(8,128)(2,1)S(1)}, bf16[128,128]{0,1:T(8,128)(2,1)S(1)}, u32[]{:S(2)}, u32[]{:S(2)}) collective-permute-start(bf16[128,128]{0,1:T(8,128)(2,1)S(1)} %pad_maximum_fusion), channel_id=1, source_target_pairs={{0,2},{2,4},{4,6},{6,8},{8,10},{10,12},{12,14},{14,16},{16,18},{18... | collective-permute-start | bytes 98312 | tf_op jit(solution)/shard_map/ppermute | solution.py:16
  11.6 0.1 subtract_convert_fusion
  11.7 0.2 fusion.22
  11.9 1.1 copy.31
  13.0 1.8 collective-permute-done
  14.8 1.6 fusion.34
  16.4 0.0 copy-done.6
  16.4 0.1 broadcast_maximum_fusion
  16.5 0.4 fusion.12
  16.9 0.1 exponential_add_fusion
  17.0 0.0 copy-done.5
  17.0 0.7 fusion.15
  17.7 0.0 copy-done
  17.7 0.0 copy-start.7
  17.7 0.0 copy-start.2
  17.8 2.1 fusion.35
  19.8 0.0 reduce-scatter.3.cloned.1.call-update
  19.9 0.0 all-gather.3.cloned.1.call-start
  19.9 0.0 copy-done.7
  19.9 0.1 copy.34
  20.0 0.1 eq.42
  20.2 0.1 eq.38
  20.3 0.6 reduce-window.6
  20.9 0.2 slice_reduce_fusion
  21.1 0.1 fusion.28
  21.2 0.1 sub.63
  21.4 0.1 copy.38
  21.5 0.1 fusion.20
  21.5 8.8 %reduce-scatter.3.cloned.1.call-done = f32[128,2048]{1,0:T(8,128)} async-done(((f32[256,2048]{1,0:T(8,128)}), f32[128,2048]{1,0:T(8,128)}) %reduce-scatter.3.cloned.1.call-update) | async-done | bytes 1048592 | tf_op jit(solution)/shard_map/reduce_scatter | solution.py:80
  30.4 0.0 copy-done.2
  30.4 1.4 multiply_reduce_fusion.1
  31.8 0.0 copy-done.4
  31.8 1.9 convolution_convert_fusion
  33.7 43.6 %all_to_all.10 = bf16[16,24,2048]{2,1,0:T(8,128)(2,1)} all-to-all(bf16[16,24,2048]{2,1,0:T(8,128)(2,1)S(1)} %bitcast.75), channel_id=1, replica_groups=mesh['sp'=16,'tp'=2] {'sp'}, dimensions={0} | all-to-all | bytes 3145728 | tf_op jit(solution)/shard_map/all_to_all | solution.py:105
  77.3 0.0 all-gather.3.cloned.1.call-update
  77.3 0.2 all-reduce.3.cloned.1.call-start
  77.5 11.4 %all-gather.3.cloned.1.call-done = bf16[16,48,2048]{2,1,0:T(8,128)(2,1)} async-done(((bf16[16,24,2048]{2,1,0:T(8,128)(2,1)}), bf16[16,48,2048]{2,1,0:T(8,128)(2,1)}) %all-gather.3.cloned.1.call-update) | async-done | bytes 3145744 | tf_op jit(solution)/shard_map/all_gather | solution.py:108
  88.9 10.0 %fusion.4 = f32[768,1792]{1,0:T(8,128)S(1)} fusion(bf16[768,2048]{1,0:T(8,128)(2,1)} %bitcast.82, bf16[1,2048,1792]{2,1,0:T(8,128)(2,1)} %param.21), kind=kOutput, calls=%fused_computation.5 | convolution fusion | flops 5637144576 | bytes 15990784 | tf_op jit(solution)/shard_map/dot_general | solution.py:112
  98.9 0.0 copy-done.9
  98.9 0.0 slice-start.1
  98.9 9.7 %multiply_convert_fusion = bf16[768,1792]{1,0:T(8,128)(2,1)S(1)} fusion(f32[768,1792]{1,0:T(8,128)S(1)} %fusion.4, bf16[768,2048]{1,0:T(8,128)(2,1)S(1)} %bitcast.83, bf16[1,2048,1792]{2,1,0:T(8,128)(2,1)} %param.22), kind=kOutput, calls=%fused_computation.7 | convolution fusion | flops 5645402112 | bytes 18743296 | tf_op jit(solution)/shard_map/dot_general | solution.py:113
  108.7 0.0 slice-done
  108.7 0.0 slice-done.1
  108.7 7.3 %fusion.8 = bf16[16,2,24,2048]{3,2,1,0:T(8,128)(2,1)} fusion(bf16[16,2,24,1792]{3,2,1,0:T(8,128)(2,1)S(1)} %bitcast.84, bf16[1,1792,2048]{2,1,0:T(8,128)(2,1)S(1)} %bitcast.81), kind=kOutput, calls=%fused_computation.8 | convolution fusion | flops 5638717440 | bytes 13238272 | tf_op jit(solution)/shard_map/dot_general | solution.py:115
  116.0 0.0 all-reduce.3.cloned.1.call-update
  116.1 0.6 copy-done.10
  116.7 0.6 dynamic-slice
  117.3 23.4 %all-reduce.3.cloned.1.call-done = bf16[16,2,24,2048]{3,2,1,0:T(8,128)(2,1)} async-done(((bf16[16,2,24,2048]{3,2,1,0:T(8,128)(2,1)}), bf16[16,2,24,2048]{3,2,1,0:T(8,128)(2,1)}) %all-reduce.3.cloned.1.call-update) | async-done | bytes 3145744
  140.7 3.4 %dynamic-slice_bitcast_fusion = bf16[16,24,2048]{2,1,0:T(8,128)(2,1)} fusion(bf16[16,2,24,2048]{3,2,1,0:T(8,128)(2,1)} %all-reduce.3.cloned.1.call-done, u32[]{:T(128)} %bitcast.29), kind=kLoop, calls=%fused_computation.16 | loop fusion | bytes 3145732 | tf_op jit(solution)/shard_map/reshape | solution.py:120
  144.1 7.0 %all-to-all-start.1 = ((bf16[16,24,2048]{2,1,0:T(8,128)(2,1)}), bf16[16,24,2048]{2,1,0:T(8,128)(2,1)}, u32[]{:S(2)}, u32[]{:S(2)}) async-start(bf16[16,24,2048]{2,1,0:T(8,128)(2,1)} %dynamic-slice_bitcast_fusion), calls=%async_computation.2 | async-start | bytes 3145728 | tf_op jit(solution)/shard_map/all_to_all | solution.py:121
  151.1 0.1 mul.117
  151.2 0.0 copy-done.8
  151.2 0.1 copy.33
  151.3 37.2 %all-to-all-done.1 = bf16[16,24,2048]{2,1,0:T(8,128)(2,1)} async-done(((bf16[16,24,2048]{2,1,0:T(8,128)(2,1)}), bf16[16,24,2048]{2,1,0:T(8,128)(2,1)}, u32[]{:S(2)}, u32[]{:S(2)}) %all-to-all-start.1) | async-done | bytes 1572896 | tf_op jit(solution)/shard_map/all_to_all | solution.py:121
  188.5 5.0 %gather_fusion = bf16[256,2048]{1,0:T(8,128)(2,1)} fusion(bf16[384,2048]{1,0:T(8,128)(2,1)} %bitcast.19, s32[1024]{0:T(1024)S(1)} %pad_clamp_fusion), kind=kCustom, calls=%fused_computation | custom fusion | bytes 2098176 | tf_op jit(solution)/shard_map/gather | solution.py:122
  193.5 3.5 %reshape.286 = f32[128,2,2048]{2,1,0:T(2,128)} reshape(bf16[256,2048]{1,0:T(8,128)(2,1)} %gather_fusion) | data formatting | bytes 3145728 | tf_op jit(solution)/shard_map/convert_element_type | solution.py:125
  197.0 4.9 %multiply_reduce_fusion = f32[128,2048]{1,0:T(8,128)S(1)} fusion(f32[128,2,2048]{2,1,0:T(2,128)} %reshape.286, f32[128,2]{1,0:T(8,128)S(1)} %copy.33), kind=kLoop, calls=%fused_computation.15 | loop fusion | flops 786432 | bytes 3146752 | tf_op jit(solution)/shard_map/reduce_sum | solution.py:125
  201.9 0.0 copy-done.1
  201.9 0.0 copy-done.3
  201.9 1.0 add_convert_fusion
  (24 shorter events, 0.1 us)
Async XLA Ops:
  6.5 11.2 %copy-start = (bf16[512,2048]{1,0:T(8,128)(2,1)S(1)}, bf16[512,2048]{1,0:T(8,128)(2,1)}, u32[]{:S(2)}) copy-start(bf16[512,2048]{1,0:T(8,128)(2,1)} %param.16) | copy-start | bytes 6291460
  6.5 9.9 %copy-start.6 = (f32[8]{0:T(128)S(1)}, f32[8]{0:T(128)}, u32[]{:S(2)}) copy-start(f32[8]{0:T(128)} %param.15) | copy-start | bytes 100
  6.5 23.8 %reduce-scatter.3.cloned.1.call-start = ((), (), s32[]{:S(2)}) async-start(), calls=%async_computation.3 | async-start | bytes 3145728 | tf_op jit(solution)/shard_map/reduce_scatter | solution.py:80
  8.1 6.7 %collective-permute-start = (bf16[128,128]{0,1:T(8,128)(2,1)S(1)}, bf16[128,128]{0,1:T(8,128)(2,1)S(1)}, u32[]{:S(2)}, u32[]{:S(2)}) collective-permute-start(bf16[128,128]{0,1:T(8,128)(2,1)S(1)} %pad_maximum_fusion), channel_id=1, source_target_pairs={{0,2},{2,4},{4,6},{6,8},{8,10},{10,12},{12,14},{14,16},{16,18},{18... | collective-permute-start | bytes 98312 | tf_op jit(solution)/shard_map/ppermute | solution.py:16
  14.8 2.2 %copy-start.5 = (bf16[256,64]{0,1:T(8,128)(2,1)S(1)}, bf16[256,64]{0,1:T(8,128)(2,1)}, u32[]{:S(2)}) copy-start(bf16[256,64]{0,1:T(8,128)(2,1)} %param.14) | copy-start | bytes 98308
  17.7 2.2 %copy-start.7 = (s32[128,2]{0,1:T(2,128)S(1)}, s32[128,2]{0,1:T(2,128)}, u32[]{:S(2)}) copy-start(s32[128,2]{0,1:T(2,128)} %param.19) | copy-start | bytes 3076
  17.7 12.6 %copy-start.2 = (bf16[128,2048]{1,0:T(8,128)(2,1)S(1)}, bf16[128,2048]{1,0:T(8,128)(2,1)}, u32[]{:S(2)}) copy-start(bf16[128,2048]{1,0:T(8,128)(2,1)} %param.17) | copy-start | bytes 1572868
  19.8 12.0 %copy-start.4 = (f32[2048]{0:T(1024)S(1)}, f32[2048]{0:T(1024)}, u32[]{:S(2)}) copy-start(f32[2048]{0:T(1024)} %param.18) | copy-start | bytes 24580
  19.9 69.0 %all-gather.3.cloned.1.call-start = ((), (), s32[]{:S(2)}) async-start(), calls=%async_computation.4 | async-start | bytes 4718592 | tf_op jit(solution)/shard_map/all_gather | solution.py:108
  77.3 63.4 %all-reduce.3.cloned.1.call-start = ((), (), s32[]{:S(2)}) async-start(), calls=%async_computation.5 | async-start | bytes 6291456
  88.9 10.0 %copy-start.9 = (bf16[16,48,2048]{2,1,0:T(8,128)(2,1)S(1)}, bf16[16,48,2048]{2,1,0:T(8,128)(2,1)}, u32[]{:S(2)}) copy-start(bf16[16,48,2048]{2,1,0:T(8,128)(2,1)} %all-gather.3.cloned.1.call-done) | copy-start | bytes 9437188
  88.9 19.8 %slice-start = ((s8[7340032]{0:T(1024)(128)(4,1)}), s8[4194304]{0:T(1024)(128)(4,1)S(1)}, s32[]{:S(2)}) async-start(s8[7340032]{0:T(1024)(128)(4,1)} %bitcast.80), calls=%async_computation.6 | async-start | bytes 8388608
  98.9 9.7 %slice-start.1 = ((s8[7340032]{0:T(1024)(128)(4,1)}), s8[3145728]{0:T(1024)(128)(4,1)S(1)}, s32[]{:S(2)}) async-start(s8[7340032]{0:T(1024)(128)(4,1)} %bitcast.80), calls=%async_computation.7 | async-start | bytes 6291456
  116.0 0.7 copy-start.10
  140.7 10.5 %copy-start.8 = (f32[128,2]{0,1:T(2,128)S(1)}, f32[128,2]{0,1:T(2,128)}, u32[]{:S(2)}) copy-start(f32[128,2]{0,1:T(2,128)} %param.20) | copy-start | bytes 3076
  144.1 44.5 %all-to-all-start.1 = ((bf16[16,24,2048]{2,1,0:T(8,128)(2,1)}), bf16[16,24,2048]{2,1,0:T(8,128)(2,1)}, u32[]{:S(2)}, u32[]{:S(2)}) async-start(bf16[16,24,2048]{2,1,0:T(8,128)(2,1)} %dynamic-slice_bitcast_fusion), calls=%async_computation.2 | async-start | bytes 3145728 | tf_op jit(solution)/shard_map/all_to_all | solution.py:121
  193.5 8.4 %copy-start.1 = (f32[128,2048]{1,0:T(8,128)S(1)}, f32[128,2048]{1,0:T(8,128)}, u32[]{:S(2)}) copy-start(f32[128,2048]{1,0:T(8,128)} %reduce-scatter.3.cloned.1.call-done) | copy-start | bytes 3145732
  197.0 4.9 %copy-start.3 = (bf16[128,2048]{1,0:T(8,128)(2,1)S(1)}, bf16[128,2048]{1,0:T(8,128)(2,1)}, u32[]{:S(2)}) copy-start(bf16[128,2048]{1,0:T(8,128)(2,1)} %param.17) | copy-start | bytes 1572868
Sparse Core Ops, SparseCore 0:
  20.0 10.3 reduce-scatter.2
  77.4 11.4 all-gather.2
  116.2 24.4 all-reduce.2
where the time goes:
time: 210 us; the launch traced here: 209 us
  waiting for transfers between devices  82.7 us (39%)
  blocking collectives  43.6 us (21%)
  matrix products  33.3 us (16%)
  local copies, waits for them, and re-layouts  16.8 us (8%)
  between operations  13.4 us (6%)
  starting transfers between devices  10.6 us (5%)
  other arithmetic  9.03 us (4%)
    all_to_all x1, blocking collectives, on_device(): lax.all_to_all(dispatch.reshape(n_sp, capacity, model_width), 'sp', split...  43.6 us
    all_to_all x1, waiting for transfers between devices, on_device(): lax.all_to_all(expert_out, 'sp', split_axis=0, concat_axis=0, tiled=True)  37.2 us
    unnamed x4, waiting for transfers between devices  23.5 us
    all_gather x1, waiting for transfers between devices, on_device(): lax.all_gather(landed.reshape(n_sp, 1, capacity, model_width), 'tp', axis...  11.4 us
    dot_general x1, matrix products, on_device(): gate = jnp.dot(rows_in, gate_proj[0], preferred_element_type=jnp.float32)  10 us
    dot_general x1, matrix products, on_device(): upper = jnp.dot(rows_in, up_proj[0], preferred_element_type=jnp.float32)  9.71 us
    reduce_scatter x1, waiting for transfers between devices, on_device(): lax.psum_scatter(jnp.dot(attended, out_weight, preferred_element_type=jnp...  8.81 us
    dot_general x1, matrix products, on_device(): jnp.dot(hidden, down_proj[0], preferred_element_type=jnp.float32)  7.35 us
  transfers between devices with their start and end apart: 5, of which 5 were waited for; matrix products, arithmetic and copies ran while one was open for 2% of the time, Pallas kernels for 0%

commit v1 on v0

--- a/solution.py
+++ b/solution.py
@@ -105,8 +105,8 @@
     landed = lax.all_to_all(
         dispatch.reshape(n_sp, capacity, model_width), "sp", split_axis=0, concat_axis=0, tiled=True
     )
-    arrived = lax.all_gather(
-        landed.reshape(n_sp, 1, capacity, model_width), "tp", axis=1, tiled=True
+    arrived = jnp.concatenate(
+        lax.all_gather(landed.reshape(n_sp, 1, capacity, model_width), "tp"), axis=1
     )
     rows_in = arrived.reshape(-1, model_width)
     gate = jnp.dot(rows_in, gate_proj[0], preferred_element_type=jnp.float32)

time: 210 us -> 208 us (level)
  matrix products: 33.3 us -> 29.1 us
  local copies, waits for them, and re-layouts: 16.8 us -> 19.1 us
    dot_general x1, matrix products: 9.71 us -> 6.43 us  [on_device(): upper = jnp.dot(rows_in, up_proj[0], preferred_element_type=jnp.float32)]
    reshape x0 -> x1, local copies, waits for them, and re-layouts: none -> 2.26 us  [on_device(): jnp.concatenate(lax.all_gather(landed.reshape(n_sp, 1, capacity, model_wi...]
where the time goes in v1:
time: 208 us
  waiting for transfers between devices  82.7 us (40%)
  blocking collectives  43.6 us (21%)
  matrix products  29.1 us (14%)
  local copies, waits for them, and re-layouts  19.1 us (9%)
  between operations  13.4 us (6%)
  starting transfers between devices  10.6 us (5%)
  other arithmetic  9.03 us (4%)
    all_to_all x1, blocking collectives, on_device(): lax.all_to_all(dispatch.reshape(n_sp, capacity, model_width), 'sp', split...  43.6 us
    all_to_all x1, waiting for transfers between devices, on_device(): lax.all_to_all(expert_out, 'sp', split_axis=0, concat_axis=0, tiled=True)  37.2 us
    unnamed x4, waiting for transfers between devices  23.5 us
    all_gather x1, waiting for transfers between devices, on_device(): lax.all_gather(landed.reshape(n_sp, 1, capacity, model_width), 'tp')  11.4 us
    dot_general x1, matrix products, on_device(): gate = jnp.dot(rows_in, gate_proj[0], preferred_element_type=jnp.float32)  9.08 us
    reduce_scatter x1, waiting for transfers between devices, on_device(): lax.psum_scatter(jnp.dot(attended, out_weight, preferred_element_type=jnp...  8.81 us
    dot_general x1, matrix products, on_device(): jnp.dot(hidden, down_proj[0], preferred_element_type=jnp.float32)  7.39 us
    all_to_all x1, starting transfers between devices, on_device(): lax.all_to_all(expert_out, 'sp', split_axis=0, concat_axis=0, tiled=True)  6.96 us
  transfers between devices with their start and end apart: 5, of which 5 were waited for; matrix products, arithmetic and copies ran while one was open for 2% of the time, Pallas kernels for 0%

profile of v1, /device:TPU:12, one launch (start us, length us, event | category | flops | bytes accessed | tf_op | source)
XLA Modules:
  0.0 207.5 jit_solution(2342490488179488316)
XLA Ops:
  6.5 0.0 copy-start
  6.5 0.0 reduce-scatter.3.cloned.1.call-start
  6.5 0.9 slice.18
  7.4 0.7 slice.19
  8.1 3.4 %collective-permute-start = (bf16[128,128]{0,1:T(8,128)(2,1)S(1)}, bf16[128,128]{0,1:T(8,128)(2,1)S(1)}, u32[]{:S(2)}, u32[]{:S(2)}) collective-permute-start(bf16[128,128]{0,1:T(8,128)(2,1)S(1)} %pad_maximum_fusion), channel_id=1, source_target_pairs={{0,2},{2,4},{4,6},{6,8},{8,10},{10,12},{12,14},{14,16},{16,18},{18... | collective-permute-start | bytes 98312 | tf_op jit(solution)/shard_map/ppermute | solution.py:16
  11.6 0.1 subtract_convert_fusion
  11.7 0.2 fusion.22
  11.9 1.1 copy.40
  13.0 1.8 collective-permute-done
  14.8 1.6 fusion.34
  16.4 0.0 copy-done.6
  16.4 0.1 broadcast_maximum_fusion
  16.5 0.4 fusion.12
  16.9 0.1 exponential_add_fusion
  17.0 0.0 copy-done.5
  17.0 0.7 fusion.15
  17.7 0.0 copy-done
  17.7 0.0 copy-start.7
  17.7 0.0 copy-start.2
  17.8 2.1 %fusion.35 = f32[256,2048]{1,0:T(8,128)} fusion(bf16[256,512]{0,1:T(8,128)(2,1)S(1)} %bitcast.82, bf16[512,2048]{1,0:T(8,128)(2,1)S(1)} %copy-done), kind=kOutput, calls=%fused_computation.64 | convolution fusion | flops 536870912 | bytes 4456448 | tf_op jit(solution)/shard_map/dot_general | solution.py:81
  19.8 0.0 reduce-scatter.3.cloned.1.call-update
  19.9 0.0 all-gather.3.cloned.1.call-start
  19.9 0.0 copy-done.7
  19.9 0.1 copy.43
  20.0 0.1 eq.42
  20.2 0.1 eq.38
  20.3 0.6 reduce-window.6
  20.9 0.2 slice_reduce_fusion
  21.1 0.1 fusion.28
  21.2 0.1 sub.63
  21.4 0.1 copy.47
  21.5 0.1 fusion.20
  21.5 8.8 %reduce-scatter.3.cloned.1.call-done = f32[128,2048]{1,0:T(8,128)} async-done(((f32[256,2048]{1,0:T(8,128)}), f32[128,2048]{1,0:T(8,128)}) %reduce-scatter.3.cloned.1.call-update) | async-done | bytes 1048592 | tf_op jit(solution)/shard_map/reduce_scatter | solution.py:80
  30.4 0.0 copy-done.2
  30.4 1.4 multiply_reduce_fusion.1
  31.8 0.0 copy-done.4
  31.8 1.9 convolution_convert_fusion
  33.7 43.6 %all_to_all.10 = bf16[16,24,2048]{2,1,0:T(8,128)(2,1)} all-to-all(bf16[16,24,2048]{2,1,0:T(8,128)(2,1)S(1)} %bitcast.78), channel_id=1, replica_groups=mesh['sp'=16,'tp'=2] {'sp'}, dimensions={0} | all-to-all | bytes 3145728 | tf_op jit(solution)/shard_map/all_to_all | solution.py:105
  77.3 0.0 all-gather.3.cloned.1.call-update
  77.3 0.2 all-reduce.3.cloned.1.call-start
  77.5 11.4 %all-gather.3.cloned.1.call-done = bf16[32,24,2048]{2,1,0:T(8,128)(2,1)} async-done(((bf16[16,24,2048]{2,1,0:T(8,128)(2,1)}), bf16[32,24,2048]{2,1,0:T(8,128)(2,1)}) %all-gather.3.cloned.1.call-update) | async-done | bytes 3145744 | tf_op jit(solution)/shard_map/all_gather | solution.py:109
  88.9 2.3 %copy.48 = bf16[16,2,1,24,2048]{4,3,1,0,2:T(8,128)(2,1)S(1)} copy(bf16[16,2,1,24,2048]{4,3,0,1,2:T(8,128)(2,1)} %bitcast.79) | data formatting | bytes 6291456 | tf_op jit(solution)/shard_map/reshape | solution.py:108
  91.2 0.0 slice-start.1
  91.2 0.0 slice-start.2
  91.2 9.1 %fusion.4 = f32[768,1792]{1,0:T(8,128)S(1)} fusion(bf16[768,2048]{1,0:T(8,128)(2,1)S(1)} %bitcast.80, bf16[1,2048,1792]{2,1,0:T(8,128)(2,1)} %param.21), kind=kOutput, calls=%fused_computation.5 | convolution fusion | flops 5637144576 | bytes 15990784 | tf_op jit(solution)/shard_map/dot_general | solution.py:112
  100.3 0.0 slice-done
  100.3 0.0 slice-start.3
  100.3 6.4 %multiply_convert_fusion = bf16[768,1792]{1,0:T(8,128)(2,1)S(1)} fusion(f32[768,1792]{1,0:T(8,128)S(1)} %fusion.4, bf16[768,2048]{1,0:T(8,128)(2,1)S(1)} %bitcast.81, bf16[1,2048,1792]{2,1,0:T(8,128)(2,1)S(1)} %bitcast.87), kind=kOutput, calls=%fused_computation.7 | convolution fusion | flops 5645402112 | bytes 18743296 | tf_op jit(solution)/shard_map/dot_general | solution.py:113
  106.8 0.0 slice-done.2
  106.8 0.0 slice-done.3
  106.8 7.4 %fusion.8 = bf16[16,2,24,2048]{3,2,1,0:T(8,128)(2,1)} fusion(bf16[16,2,24,1792]{3,2,1,0:T(8,128)(2,1)S(1)} %bitcast.90, bf16[1,1792,2048]{2,1,0:T(8,128)(2,1)S(1)} %bitcast.89), kind=kOutput, calls=%fused_computation.8 | convolution fusion | flops 5638717440 | bytes 13238272 | tf_op jit(solution)/shard_map/dot_general | solution.py:115
  114.2 0.0 all-reduce.3.cloned.1.call-update
  114.2 0.6 copy-done.9
  114.8 0.6 dynamic-slice
  115.4 23.4 %all-reduce.3.cloned.1.call-done = bf16[16,2,24,2048]{3,2,1,0:T(8,128)(2,1)} async-done(((bf16[16,2,24,2048]{3,2,1,0:T(8,128)(2,1)}), bf16[16,2,24,2048]{3,2,1,0:T(8,128)(2,1)}) %all-reduce.3.cloned.1.call-update) | async-done | bytes 3145744
  138.8 3.4 %dynamic-slice_bitcast_fusion = bf16[16,24,2048]{2,1,0:T(8,128)(2,1)} fusion(bf16[16,2,24,2048]{3,2,1,0:T(8,128)(2,1)} %all-reduce.3.cloned.1.call-done, u32[]{:T(128)} %bitcast.32), kind=kLoop, calls=%fused_computation.16 | loop fusion | bytes 3145732 | tf_op jit(solution)/shard_map/reshape | solution.py:120
  142.2 7.0 %all-to-all-start.1 = ((bf16[16,24,2048]{2,1,0:T(8,128)(2,1)}), bf16[16,24,2048]{2,1,0:T(8,128)(2,1)}, u32[]{:S(2)}, u32[]{:S(2)}) async-start(bf16[16,24,2048]{2,1,0:T(8,128)(2,1)} %dynamic-slice_bitcast_fusion), calls=%async_computation.2 | async-start | bytes 3145728 | tf_op jit(solution)/shard_map/all_to_all | solution.py:121
  149.2 0.1 mul.117
  149.4 0.1 copy.42
  149.5 37.2 %all-to-all-done.1 = bf16[16,24,2048]{2,1,0:T(8,128)(2,1)} async-done(((bf16[16,24,2048]{2,1,0:T(8,128)(2,1)}), bf16[16,24,2048]{2,1,0:T(8,128)(2,1)}, u32[]{:S(2)}, u32[]{:S(2)}) %all-to-all-start.1) | async-done | bytes 1572896 | tf_op jit(solution)/shard_map/all_to_all | solution.py:121
  186.7 5.0 %gather_fusion = bf16[256,2048]{1,0:T(8,128)(2,1)} fusion(bf16[384,2048]{1,0:T(8,128)(2,1)} %bitcast.21, s32[1024]{0:T(1024)S(1)} %pad_clamp_fusion), kind=kCustom, calls=%fused_computation | custom fusion | bytes 2098176 | tf_op jit(solution)/shard_map/gather | solution.py:122
  191.7 3.5 %reshape.282 = f32[128,2,2048]{2,1,0:T(2,128)} reshape(bf16[256,2048]{1,0:T(8,128)(2,1)} %gather_fusion) | data formatting | bytes 3145728 | tf_op jit(solution)/shard_map/convert_element_type | solution.py:125
  195.1 4.9 %multiply_reduce_fusion = f32[128,2048]{1,0:T(8,128)S(1)} fusion(f32[128,2,2048]{2,1,0:T(2,128)} %reshape.282, f32[128,2]{1,0:T(8,128)S(1)} %copy.42), kind=kLoop, calls=%fused_computation.15 | loop fusion | flops 786432 | bytes 3146752 | tf_op jit(solution)/shard_map/reduce_sum | solution.py:125
  200.0 1.0 add_convert_fusion
  (28 shorter events, 0.1 us)
Async XLA Ops:
  6.5 11.2 %copy-start = (bf16[512,2048]{1,0:T(8,128)(2,1)S(1)}, bf16[512,2048]{1,0:T(8,128)(2,1)}, u32[]{:S(2)}) copy-start(bf16[512,2048]{1,0:T(8,128)(2,1)} %param.16) | copy-start | bytes 6291460
  6.5 9.9 %copy-start.6 = (f32[8]{0:T(128)S(1)}, f32[8]{0:T(128)}, u32[]{:S(2)}) copy-start(f32[8]{0:T(128)} %param.15) | copy-start | bytes 100
  6.5 23.8 %reduce-scatter.3.cloned.1.call-start = ((), (), s32[]{:S(2)}) async-start(), calls=%async_computation.3 | async-start | bytes 3145728 | tf_op jit(solution)/shard_map/reduce_scatter | solution.py:80
  8.1 6.7 %collective-permute-start = (bf16[128,128]{0,1:T(8,128)(2,1)S(1)}, bf16[128,128]{0,1:T(8,128)(2,1)S(1)}, u32[]{:S(2)}, u32[]{:S(2)}) collective-permute-start(bf16[128,128]{0,1:T(8,128)(2,1)S(1)} %pad_maximum_fusion), channel_id=1, source_target_pairs={{0,2},{2,4},{4,6},{6,8},{8,10},{10,12},{12,14},{14,16},{16,18},{18... | collective-permute-start | bytes 98312 | tf_op jit(solution)/shard_map/ppermute | solution.py:16
  14.8 2.2 %copy-start.5 = (bf16[256,64]{0,1:T(8,128)(2,1)S(1)}, bf16[256,64]{0,1:T(8,128)(2,1)}, u32[]{:S(2)}) copy-start(bf16[256,64]{0,1:T(8,128)(2,1)} %param.14) | copy-start | bytes 98308
  17.7 2.2 %copy-start.7 = (s32[128,2]{0,1:T(2,128)S(1)}, s32[128,2]{0,1:T(2,128)}, u32[]{:S(2)}) copy-start(s32[128,2]{0,1:T(2,128)} %param.19) | copy-start | bytes 3076
  17.7 12.6 %copy-start.2 = (bf16[128,2048]{1,0:T(8,128)(2,1)S(1)}, bf16[128,2048]{1,0:T(8,128)(2,1)}, u32[]{:S(2)}) copy-start(bf16[128,2048]{1,0:T(8,128)(2,1)} %param.17) | copy-start | bytes 1572868
  19.8 12.0 %copy-start.4 = (f32[2048]{0:T(1024)S(1)}, f32[2048]{0:T(1024)}, u32[]{:S(2)}) copy-start(f32[2048]{0:T(1024)} %param.18) | copy-start | bytes 24580
  19.9 69.0 %all-gather.3.cloned.1.call-start = ((), (), s32[]{:S(2)}) async-start(), calls=%async_computation.4 | async-start | bytes 4718592 | tf_op jit(solution)/shard_map/all_gather | solution.py:109
  77.3 61.5 %all-reduce.3.cloned.1.call-start = ((), (), s32[]{:S(2)}) async-start(), calls=%async_computation.5 | async-start | bytes 6291456
  88.9 11.4 %slice-start = ((s8[7340032]{0:T(1024)(128)(4,1)}), s8[4194304]{0:T(1024)(128)(4,1)S(1)}, s32[]{:S(2)}) async-start(s8[7340032]{0:T(1024)(128)(4,1)} %bitcast.86), calls=%async_computation.6 | async-start | bytes 8388608
  91.2 9.1 %slice-start.1 = ((s8[7340032]{0:T(1024)(128)(4,1)}), s8[3145728]{0:T(1024)(128)(4,1)S(1)}, s32[]{:S(2)}) async-start(s8[7340032]{0:T(1024)(128)(4,1)} %bitcast.86), calls=%async_computation.7 | async-start | bytes 6291456
  91.2 15.6 %slice-start.2 = ((s8[7340032]{0:T(1024)(128)(4,1)}), s8[4194304]{0:T(1024)(128)(4,1)S(1)}, s32[]{:S(2)}) async-start(s8[7340032]{0:T(1024)(128)(4,1)} %bitcast.88), calls=%async_computation.8 | async-start | bytes 8388608
  100.3 6.5 %slice-start.3 = ((s8[7340032]{0:T(1024)(128)(4,1)}), s8[3145728]{0:T(1024)(128)(4,1)S(1)}, s32[]{:S(2)}) async-start(s8[7340032]{0:T(1024)(128)(4,1)} %bitcast.88), calls=%async_computation.9 | async-start | bytes 6291456
  114.2 0.7 copy-start.9
  138.8 10.5 %copy-start.8 = (f32[128,2]{0,1:T(2,128)S(1)}, f32[128,2]{0,1:T(2,128)}, u32[]{:S(2)}) copy-start(f32[128,2]{0,1:T(2,128)} %param.20) | copy-start | bytes 3076
  142.2 44.5 %all-to-all-start.1 = ((bf16[16,24,2048]{2,1,0:T(8,128)(2,1)}), bf16[16,24,2048]{2,1,0:T(8,128)(2,1)}, u32[]{:S(2)}, u32[]{:S(2)}) async-start(bf16[16,24,2048]{2,1,0:T(8,128)(2,1)} %dynamic-slice_bitcast_fusion), calls=%async_computation.2 | async-start | bytes 3145728 | tf_op jit(solution)/shard_map/all_to_all | solution.py:121
  191.7 8.3 %copy-start.1 = (f32[128,2048]{1,0:T(8,128)S(1)}, f32[128,2048]{1,0:T(8,128)}, u32[]{:S(2)}) copy-start(f32[128,2048]{1,0:T(8,128)} %reduce-scatter.3.cloned.1.call-done) | copy-start | bytes 3145732
  195.1 4.9 %copy-start.3 = (bf16[128,2048]{1,0:T(8,128)(2,1)S(1)}, bf16[128,2048]{1,0:T(8,128)(2,1)}, u32[]{:S(2)}) copy-start(bf16[128,2048]{1,0:T(8,128)(2,1)} %param.17) | copy-start | bytes 1572868
Sparse Core Ops, SparseCore 0:
  20.0 10.3 reduce-scatter.2
  77.4 11.4 all-gather.2
  114.3 24.4 all-reduce.2
